TPU v7x, 512 devices: a whole 4x4x16 slice. The times are simulated.
512 devices in a mesh: sp: 128 (over z, x, core), tp: 4 (over y).
Axes of the slice: x: 4, y: 4, z: 16, core: 2. Of those that a mesh axis runs over, the one named last changes fastest.
Arguments:
- tokens: bfloat16 [16384, 2048], P(('sp', 'tp')), may hold values from -6 to 6
- input_norm_gain: float32 [2048], replicated, may hold values from 0.1 to 1.9
- convolution_value_weight: bfloat16 [2048, 1024], P('sp', 'tp'), may hold values from -0.125 to 0.125
- convolution_gate_weight: bfloat16 [2048, 1024], P('sp', 'tp'), may hold values from -0.125 to 0.125
- depthwise_filter_taps: float32 [31, 1024], P(None, 'tp'), may hold values from -4 to 4
- channel_norm_gain: float32 [1024], P('tp'), may hold values from 0.1 to 1.9
- channel_norm_bias: float32 [1024], P('tp'), may hold values from -3 to 3
- query_projection_weight: bfloat16 [2048, 1024], P('sp', 'tp'), may hold values from -0.125 to 0.125
- forget_gate_weight: bfloat16 [2048, 1024], P('sp', 'tp'), may hold values from -0.125 to 0.125
- recurrence_value_weight: bfloat16 [2048, 1024], P('sp', 'tp'), may hold values from -0.125 to 0.125
- output_gate_weight: bfloat16 [2048, 1024], P('sp', 'tp'), may hold values from -0.125 to 0.125
- forget_floor_margin: float32 [1024], P('tp'), may hold values from 6.1035156e-06 to 0.1
- decay_jump_terms: float32 [8, 16384], P('tp', 'sp'), may hold values from -0.7 to 0
- head_norm_gain: float32 [1024], P('tp'), may hold values from 0.1 to 1.9
- convolution_output_weight: bfloat16 [1024, 2048], P('tp', 'sp'), may hold values from -0.125 to 0.125
- recurrence_output_weight: bfloat16 [1024, 2048], P('tp', 'sp'), may hold values from -0.125 to 0.125
Outputs:
- mixed: bfloat16 [16384, 2048], P(('sp', 'tp'))
All inputs are finite; a program needn't handle non-finite values.
Results may differ from a plain program's by a relative error of at most 0.015.
Values may be sent and summed in bfloat16 or wider, within the bound.
A program may use at most 64 MiB of HBM per device.

v0:
```python
import jax
import jax.numpy as jnp
from jax import lax
from jax.sharding import Mesh
from jax.sharding import PartitionSpec as P

CONV_CH = 1024
HG_DK = 128
HG_DV = 128
HG_BLOCK = 64
SP = ("sp_0", "sp_1", "sp_2")
SP_TP = ("sp_0", "sp_1", "sp_2", "tp")


norm_eps = 1e-06
layer_eps = 1e-05


def rows_first(arrays, axis, dims):
    turned = [jnp.moveaxis(a, dim, 0) for a, dim in zip(arrays, dims)]
    both = jnp.concatenate([t.reshape(len(t), -1) for t in turned], axis=1)
    out, at, outs = (lax.all_gather(both, axis, axis=0, tiled=True), 0, [])
    for t, dim in zip(turned, dims):
        section = out[:, at : at + t[0].size].reshape(-1, *t.shape[1:])
        outs.append(jnp.moveaxis(section, 0, dim))
        at += t[0].size
    return tuple(outs)


def joined_along(blocks, dim):
    shape = list(blocks.shape[1:])
    shape[dim] *= blocks.shape[0]
    return jnp.moveaxis(blocks, 0, dim).reshape(shape)


def sent_to_all(x, axis):
    copies = jnp.broadcast_to(x, (lax.axis_size(axis), *x.shape))
    return lax.all_to_all(copies, axis, split_axis=0, concat_axis=0, tiled=True)


def gather_directly(x, axis, dim):
    return joined_along(sent_to_all(x, axis), dim)


def passed_along(value, axis, steps):
    count = lax.axis_size(axis)
    initial, last = (max(0, -steps), min(count, count - steps))
    return lax.ppermute(value, axis, [(source, source + steps) for source in range(initial, last)])


def filled_with(x, identity):
    return jax.tree.map(
        lambda part, zero: jnp.zeros_like(part) + jnp.asarray(zero, part.dtype), x, identity
    )


def entering(x, axes, combine, identity):
    before = start = filled_with(x, identity)
    running = x
    for axis in reversed(axes):
        size, mine = (lax.axis_size(axis), lax.axis_index(axis))
        pieces = jax.tree.map(
            lambda part, kind: lax.all_gather(part.astype(kind), axis),
            running,
            (jnp.bfloat16, jnp.bfloat16),
        )
        inside, running = (start, start)
        for k in range(size):
            passed = k < mine
            running = combine(
                running, jax.tree.map(lambda part, own: part[k].astype(own.dtype), pieces, x)
            )
            inside = jax.tree.map(lambda new, old: jnp.where(passed, new, old), running, inside)
        before = combine(inside, before)
    return before


def of_everyone(x, axis):
    return sent_to_all(x, axis).sum(axis=0)


def together(arrays, axis):
    flat, at, outs = (jnp.concatenate([a.reshape(-1) for a in arrays]), 0, [])
    running = of_everyone(flat, axis)
    for a in arrays:
        outs.append(running[at : at + a.size].reshape(a.shape))
        at += a.size
    return tuple(outs)


def in_blocks(x, dim, size):
    shape = x.shape
    blocks = x.reshape(*shape[:dim], size, shape[dim] // size, *shape[dim + 1 :])
    return jnp.moveaxis(blocks, dim, 0)


def sent_and_summed(x, axis, dim):
    blocks = in_blocks(x, dim, lax.axis_size(axis))
    arrived = lax.all_to_all(blocks, axis, split_axis=0, concat_axis=0, tiled=True)
    return arrived.astype(jnp.float32).sum(axis=0)


def convolve(gated, kernel):
    return lax.conv_general_dilated(
        gated[None],
        kernel[:, None, :],
        (1,),
        "VALID",
        dimension_numbers=("NWC", "WIO", "NWC"),
        feature_group_count=gated.shape[1],
    )[0]


def channel_norm(values, first_sum, second_sum, gain, bias):
    mean_value = first_sum[:, None] / CONV_CH
    variance = second_sum[:, None] / CONV_CH - mean_value * mean_value
    shifted = (values - mean_value) * lax.rsqrt(variance + layer_eps) * gain + bias
    return jax.nn.silu(shifted).astype(jnp.bfloat16)


def gate_factors(query_projected, forget_projected, forget_floor_margin, decay_jump_rows):
    row_total_count = query_projected.shape[0]
    head_total_count = decay_jump_rows.shape[1]
    query_rows = jax.nn.silu(query_projected.astype(jnp.float32))
    log_forget_gate = jnp.logaddexp(
        jnp.log1p(-forget_floor_margin),
        jnp.log(forget_floor_margin) + jax.nn.log_sigmoid(forget_projected.astype(jnp.float32)),
    )
    key_gate_values = -jnp.expm1(log_forget_gate)
    log_decay_running = (
        log_forget_gate.reshape(row_total_count, head_total_count, -1) + decay_jump_rows[:, :, None]
    )
    return (
        query_rows.reshape(row_total_count, head_total_count, -1),
        key_gate_values.reshape(row_total_count, head_total_count, -1),
        log_decay_running,
    )


def finish(recurrent, gain, outgate_proj):
    row_total_count = recurrent.shape[0]
    scaled = recurrent * lax.rsqrt(
        jnp.mean(recurrent * recurrent, axis=2, keepdims=True) + norm_eps
    )
    gated_out = (
        scaled.reshape(row_total_count, -1) * gain * jax.nn.silu(outgate_proj.astype(jnp.float32))
    )
    return gated_out.astype(jnp.bfloat16)


def combine_states(first_part, second_part):
    return (
        first_part[0] + second_part[0],
        jnp.exp(second_part[0])[:, :, None] * first_part[1] + second_part[1],
    )


def carry_step(recurrence_state, block_parts):
    decay_end, contribution = block_parts
    return (jnp.exp(decay_end)[:, :, None] * recurrence_state + contribution, recurrence_state)


def per_device(
    tokens,
    input_norm_gain,
    convolution_value_weight,
    convolution_gate_weight,
    depthwise_filter_taps,
    channel_norm_gain,
    channel_norm_bias,
    query_projection_weight,
    forget_gate_weight,
    recurrence_value_weight,
    output_gate_weight,
    forget_floor_margin,
    decay_jump_terms,
    head_norm_gain,
    convolution_output_weight,
    recurrence_output_weight,
):
    features = tokens.astype(jnp.float32)
    normed = (
        features
        * lax.rsqrt(jnp.mean(features * features, axis=1, keepdims=True) + norm_eps)
        * input_norm_gain
    ).astype(jnp.bfloat16)
    gathered = rows_first(
        (
            convolution_value_weight,
            convolution_gate_weight,
            query_projection_weight,
            forget_gate_weight,
            recurrence_value_weight,
            output_gate_weight,
            convolution_output_weight,
            recurrence_output_weight,
        ),
        SP,
        (0, 0, 0, 0, 0, 0, 1, 1),
    )
    projection_weights = gathered[:6]
    conv_columns = gathered[6]
    rec_columns = gathered[7]

    def project(row_piece):
        return jnp.concatenate(
            [
                jnp.dot(row_piece, weight, preferred_element_type=jnp.float32).astype(jnp.bfloat16)
                for weight in projection_weights
            ],
            axis=1,
        )

    projected = project(gather_directly(normed, "tp", 0))
    offsets = []
    position = 0
    for weight in projection_weights[:-1]:
        position = position + weight.shape[1]
        offsets.append(position)
    value_proj, gate_proj, query_projected, forget_projected, input_proj, outgate_proj = jnp.split(
        projected, offsets, axis=1
    )
    row_total_count = value_proj.shape[0]
    rim_rows = depthwise_filter_taps.shape[0] - 1
    tail_value, tail_gate = passed_along(
        (value_proj[row_total_count - rim_rows :], gate_proj[row_total_count - rim_rows :]), SP, 1
    )
    value_ext = jnp.concatenate([tail_value, value_proj], axis=0)
    gate_ext = jnp.concatenate([tail_gate, gate_proj], axis=0)
    gated = value_ext.astype(jnp.float32) * jax.nn.sigmoid(gate_ext.astype(jnp.float32))
    convolved = convolve(gated, depthwise_filter_taps).astype(jnp.bfloat16)
    device_heads = decay_jump_terms.shape[0]
    query_rows, key_gate_values, log_decay_running = gate_factors(
        query_projected, forget_projected, forget_floor_margin, decay_jump_terms.T
    )
    input_rows = input_proj.astype(jnp.float32).reshape(row_total_count, device_heads, -1)
    block_count = row_total_count // HG_BLOCK

    def to_blocks(array):
        return array.reshape(block_count, HG_BLOCK, device_heads, -1).transpose(0, 2, 1, 3)

    block_queries = to_blocks(query_rows)
    block_keys = to_blocks(key_gate_values)
    block_inputs = to_blocks(input_rows)
    cumulative = jnp.cumsum(to_blocks(log_decay_running), axis=2)
    final_decay = cumulative[:, :, -1, :]
    query_rows_scaled = block_queries * jnp.exp(cumulative)
    scaled_keys = block_keys * jnp.exp(-cumulative)
    final_keys = block_keys * jnp.exp(final_decay[:, :, None, :] - cumulative)
    attention_scores = jnp.einsum("nhtk,nhsk->nhts", query_rows_scaled, scaled_keys)
    causal = jnp.arange(HG_BLOCK)[:, None] >= jnp.arange(HG_BLOCK)[None, :]
    attention_scores = jnp.where(causal[None, None], attention_scores, 0.0)
    inner = jnp.einsum("nhts,nhsv->nhtv", attention_scores, block_inputs)
    contributions = jnp.einsum("nhsk,nhsv->nhkv", final_keys, block_inputs)
    initial = jnp.zeros((device_heads, HG_DK, HG_DV), jnp.float32)
    local_state, block_starts = lax.scan(carry_step, initial, (final_decay, contributions))
    device_decay = jnp.sum(final_decay, axis=0)
    before_blocks = jnp.cumsum(final_decay, axis=0) - final_decay
    incoming = entering(
        (device_decay, local_state),
        SP,
        combine_states,
        (jnp.zeros_like(device_decay), jnp.zeros_like(local_state)),
    )
    starts = block_starts + jnp.exp(before_blocks)[:, :, :, None] * incoming[1][None]
    recurrent = inner + jnp.einsum("nhtk,nhkv->nhtv", query_rows_scaled, starts)
    recurrent = recurrent.transpose(0, 2, 1, 3).reshape(row_total_count, device_heads, -1)
    rec_out = finish(recurrent, head_norm_gain, outgate_proj)
    values = convolved.astype(jnp.float32)
    totals = together((jnp.sum(values, axis=1), jnp.sum(values * values, axis=1)), "tp")
    conv_out = channel_norm(values, totals[0], totals[1], channel_norm_gain, channel_norm_bias)
    conv_part = lax.slice_in_dim(
        conv_out, 0, row_total_count // lax.axis_size("tp") * lax.axis_size("tp"), axis=0
    )
    summed = sent_and_summed(
        (
            jnp.dot(conv_part, conv_columns, preferred_element_type=jnp.float32)
            + jnp.dot(rec_out, rec_columns, preferred_element_type=jnp.float32)
        ).astype(jnp.bfloat16),
        "tp",
        0,
    )
    return summed.astype(jnp.bfloat16)


def solution(mesh):
    split = Mesh(mesh.devices.reshape(16, 4, 2, mesh.shape["tp"]), ("sp_0", "sp_1", "sp_2", "tp"))
    return jax.shard_map(
        per_device,
        mesh=split,
        in_specs=(
            P(SP_TP, None),
            P(),
            P(SP, "tp"),
            P(SP, "tp"),
            P(None, "tp"),
            P("tp"),
            P("tp"),
            P(SP, "tp"),
            P(SP, "tp"),
            P(SP, "tp"),
            P(SP, "tp"),
            P("tp"),
            P("tp", SP),
            P("tp"),
            P("tp", SP),
            P("tp", SP),
        ),
        out_specs=P(SP_TP, None),
        check_vma=False,
    )
```

profile of v0, /device:TPU:6, one launch (start us, length us, event | category | flops | bytes accessed | tf_op | source)
XLA Modules:
  0.0 284.3 jit_solution(15545226052518464159)
XLA Ops:
  6.5 0.7 constant_dynamic-update-slice_fusion.7
  7.2 0.7 constant_dynamic-update-slice_fusion.6
  7.9 0.7 constant_dynamic-update-slice_fusion.5
  8.6 0.7 constant_dynamic-update-slice_fusion.4
  9.3 0.7 constant_dynamic-update-slice_fusion.3
  10.0 0.7 constant_dynamic-update-slice_fusion.2
  10.7 0.7 constant_dynamic-update-slice_fusion.1
  11.4 0.7 constant_dynamic-update-slice_fusion
  12.1 0.6 copy-done.1
  12.8 0.0 all-gather.6.cloned.1.call-update
  12.8 1.0 fusion.18
  13.8 1.0 fusion.20
  14.9 0.9 broadcast_in_dim.27
  15.8 4.5 %all-to-all-start = ((bf16[4,32,2048]{2,1,0:T(8,128)(2,1)}), bf16[4,32,2048]{2,1,0:T(8,128)(2,1)S(1)}, u32[]{:S(2)}, u32[]{:S(2)}) async-start(bf16[4,32,2048]{2,1,0:T(8,128)(2,1)} %broadcast_in_dim.27), calls=%async_computation | async-start | bytes 1048576 | tf_op jit(solution)/shard_map/all_to_all | solution.py:38
  20.2 0.8 add.274
  21.0 0.7 negate_log-plus-one_fusion
  21.7 8.0 %all-to-all-done = bf16[4,32,2048]{2,1,0:T(8,128)(2,1)S(1)} async-done(((bf16[4,32,2048]{2,1,0:T(8,128)(2,1)}), bf16[4,32,2048]{2,1,0:T(8,128)(2,1)S(1)}, u32[]{:S(2)}, u32[]{:S(2)}) %all-to-all-start) | async-done | bytes 524320 | tf_op jit(solution)/shard_map/all_to_all | solution.py:38
  29.7 132.8 %all-gather.6.cloned.1.call-done = bf16[2048,2048]{1,0:T(8,128)(2,1)} async-done(((bf16[16,2048]{1,0:T(8,128)(2,1)}), bf16[2048,2048]{1,0:T(8,128)(2,1)}) %all-gather.6.cloned.1.call-update) | async-done | bytes 8388624 | tf_op jit(solution)/shard_map/all_gather | solution.py:22
  162.5 1.7 exponential-minus-one_negate_fusion
  164.3 0.1 reshape.413
  164.3 0.1 fusion.40
  164.4 0.1 reduce_window_sum.22
  164.6 0.1 reshape_reshape.10
  164.7 1.5 convolution_convert_fusion.2
  166.2 0.0 copy-start.2
  166.2 0.0 copy-start.3
  166.3 0.2 fusion.39
  166.5 0.4 while.13
  166.6 0.1 bitcast_add_fusion.2
  166.8 0.1 bitcast_add_fusion.2
  166.9 1.9 all-gather.1
  168.8 1.8 all-gather.2
  170.6 0.1 fusion.63
  170.8 0.0 copy-start.4
  170.8 12.3 %all_gather.35 = bf16[4,2,128,128]{3,2,1,0:T(8,128)(2,1)S(1)} all-gather(bf16[1,2,128,128]{3,2,1,0:T(8,128)(2,1)S(1)} %fusion.63), channel_id=1, replica_groups=mesh['sp_0'=16,'sp_1'=4,'sp_2'=2,'tp'=4] {'sp_1'}, dimensions={0}, use_global_device_ids=true | all-gather | bytes 327680 | tf_op jit(solution)/shard_map/all_gather | solution.py:63
  183.0 8.5 %all_gather.31 = bf16[4,2,128]{2,1,0:T(2,128)(2,1)S(1)} all-gather(bf16[1,2,128]{2,1,0:T(2,128)(2,1)S(1)} %get-tuple-element.87), channel_id=1, replica_groups=mesh['sp_0'=16,'sp_1'=4,'sp_2'=2,'tp'=4] {'sp_1'}, dimensions={0}, use_global_device_ids=true | all-gather | bytes 2560 | tf_op jit(solution)/shard_map/all_gather | solution.py:63
  191.5 0.8 fusion.46
  192.4 0.0 all-gather.8.cloned.1.call-update
  192.4 1.6 divide_multiply_fusion.1
  194.0 0.1 reshape_reshape.9
  194.0 1.5 convolution_convert_fusion.6
  195.6 1.9 collective-permute-start
  197.5 1.5 convolution_convert_fusion.5
  199.1 4.9 %collective-permute-start.1 = (bf16[30,256]{1,0:T(8,128)(2,1)S(1)}, bf16[30,256]{1,0:T(8,128)(2,1)S(1)}, u32[]{:S(2)}, u32[]{:S(2)}) collective-permute-start(bf16[30,256]{1,0:T(8,128)(2,1)S(1)} %slice.237), channel_id=1, source_target_pairs={{0,4},{4,8},{8,12},{12,16},{16,20},{20,24},{24,28},{28,32},{32,36}... | collective-permute-start | bytes 46088 | tf_op jit(solution)/shard_map/ppermute | solution.py:48
  203.9 26.1 %all_gather.32 = bf16[16,2,128]{2,1,0:T(2,128)(2,1)S(1)} all-gather(bf16[1,2,128]{2,1,0:T(2,128)(2,1)S(1)} %get-tuple-element.83), channel_id=1, replica_groups=mesh['sp_0'=16,'sp_1'=4,'sp_2'=2,'tp'=4] {'sp_0'}, dimensions={0}, use_global_device_ids=true | all-gather | bytes 8704 | tf_op jit(solution)/shard_map/all_gather | solution.py:63
  230.0 0.3 fusion.2
  230.3 0.0 collective-permute-done
  230.3 0.0 collective-permute-done.1
  230.4 0.1 divide_multiply_fusion
  230.4 2.2 fusion.97
  232.6 0.1 fusion.29
  232.8 0.6 broadcast_in_dim.29
  233.3 4.3 %all-to-all-start.1 = ((f32[4,1,256]{2,1,0:T(1,128)}), f32[4,1,256]{2,1,0:T(1,128)S(1)}, u32[]{:S(2)}, u32[]{:S(2)}) async-start(f32[4,1,256]{2,1,0:T(1,128)} %broadcast_in_dim.29), calls=%async_computation.1 | async-start | bytes 8192 | tf_op jit(solution)/shard_map/all_to_all | solution.py:38
  237.6 5.3 %all-to-all-done.1 = f32[4,1,256]{2,1,0:T(1,128)S(1)} async-done(((f32[4,1,256]{2,1,0:T(1,128)}), f32[4,1,256]{2,1,0:T(1,128)S(1)}, u32[]{:S(2)}, u32[]{:S(2)}) %all-to-all-start.1) | async-done | bytes 4128 | tf_op jit(solution)/shard_map/all_to_all | solution.py:38
  243.0 1.7 fusion.14
  244.7 14.4 %all-gather.8.cloned.1.call-done = bf16[16,2,128,128]{3,2,1,0:T(8,128)(2,1)} async-done(((bf16[1,2,128,128]{3,2,1,0:T(8,128)(2,1)}), bf16[16,2,128,128]{3,2,1,0:T(8,128)(2,1)}) %all-gather.8.cloned.1.call-update) | async-done | bytes 1048592 | tf_op jit(solution)/shard_map/all_gather | solution.py:63
  259.1 2.1 fusion.38
  261.2 0.4 multiply_reduce_fusion
  261.6 0.1 copy.64
  261.7 0.1 copy.61
  261.8 0.2 mul.422
  262.1 2.5 fusion
  264.5 12.2 %all_to_all.16 = bf16[4,32,2048]{2,1,0:T(8,128)(2,1)S(1)} all-to-all(bf16[4,32,2048]{2,1,0:T(8,128)(2,1)S(1)} %bitcast.162), channel_id=1, replica_groups=mesh['sp_0'=16,'sp_1'=4,'sp_2'=2,'tp'=4] {'tp'}, dimensions={0} | all-to-all | bytes 1048576 | tf_op jit(solution)/shard_map/all_to_all | solution.py:99
  276.7 0.7 reduce_sum.72
  (31 shorter events, 0.3 us)
Async XLA Ops:
  6.5 223.9 %copy-start = (f32[31,256]{1,0:T(8,128)S(1)}, f32[31,256]{1,0:T(8,128)}, u32[]{:S(2)}) copy-start(f32[31,256]{1,0:T(8,128)} %param.22) | copy-start | bytes 95236
  6.5 156.0 %all-gather.6.cloned.1.call-start = ((), (), s32[]{:S(2)}) async-start(), calls=%async_computation.3 | async-start | bytes 8454144 | tf_op jit(solution)/shard_map/all_gather | solution.py:22
  12.1 0.6 copy-start.1
  15.8 13.9 %all-to-all-start = ((bf16[4,32,2048]{2,1,0:T(8,128)(2,1)}), bf16[4,32,2048]{2,1,0:T(8,128)(2,1)S(1)}, u32[]{:S(2)}, u32[]{:S(2)}) async-start(bf16[4,32,2048]{2,1,0:T(8,128)(2,1)} %broadcast_in_dim.27), calls=%async_computation | async-start | bytes 1048576 | tf_op jit(solution)/shard_map/all_to_all | solution.py:38
  20.2 238.9 %all-gather.8.cloned.1.call-start = ((), (), s32[]{:S(2)}) async-start(), calls=%async_computation.4 | async-start | bytes 1114112 | tf_op jit(solution)/shard_map/all_gather | solution.py:63
  166.2 76.7 %copy-start.2 = (f32[256]{0:T(256)S(1)}, f32[256]{0:T(256)}, u32[]{:S(2)}) copy-start(f32[256]{0:T(256)} %param.24) | copy-start | bytes 3076
  166.2 76.7 %copy-start.3 = (f32[256]{0:T(256)S(1)}, f32[256]{0:T(256)}, u32[]{:S(2)}) copy-start(f32[256]{0:T(256)} %param.23) | copy-start | bytes 3076
  170.8 91.3 %copy-start.4 = (f32[256]{0:T(256)S(1)}, f32[256]{0:T(256)}, u32[]{:S(2)}) copy-start(f32[256]{0:T(256)} %param.31) | copy-start | bytes 3076
  195.6 34.7 %collective-permute-start = (bf16[30,256]{1,0:T(8,128)(2,1)S(1)}, bf16[30,256]{1,0:T(8,128)(2,1)S(1)}, u32[]{:S(2)}, u32[]{:S(2)}) collective-permute-start(bf16[30,256]{1,0:T(8,128)(2,1)S(1)} %slice.235), channel_id=1, source_target_pairs={{0,4},{4,8},{8,12},{12,16},{16,20},{20,24},{24,28},{28,32},{32,36}... | collective-permute-start | bytes 46088 | tf_op jit(solution)/shard_map/ppermute | solution.py:48
  199.1 31.3 %collective-permute-start.1 = (bf16[30,256]{1,0:T(8,128)(2,1)S(1)}, bf16[30,256]{1,0:T(8,128)(2,1)S(1)}, u32[]{:S(2)}, u32[]{:S(2)}) collective-permute-start(bf16[30,256]{1,0:T(8,128)(2,1)S(1)} %slice.237), channel_id=1, source_target_pairs={{0,4},{4,8},{8,12},{12,16},{16,20},{20,24},{24,28},{28,32},{32,36}... | collective-permute-start | bytes 46088 | tf_op jit(solution)/shard_map/ppermute | solution.py:48
  233.3 9.6 %all-to-all-start.1 = ((f32[4,1,256]{2,1,0:T(1,128)}), f32[4,1,256]{2,1,0:T(1,128)S(1)}, u32[]{:S(2)}, u32[]{:S(2)}) async-start(f32[4,1,256]{2,1,0:T(1,128)} %broadcast_in_dim.29), calls=%async_computation.1 | async-start | bytes 8192 | tf_op jit(solution)/shard_map/all_to_all | solution.py:38
Sparse Core Ops, SparseCore 0:
  12.9 149.5 all-gather.5
  192.5 66.5 all-gather.7
where the time goes:
time: 285 us; the launch traced here: 284 us
  waiting for transfers between devices  161 us (56%)
  blocking collectives  62.7 us (22%)
  starting transfers between devices  15.5 us (5%)
  matrix products  15.2 us (5%)
  between operations  13.7 us (5%)
  local copies, waits for them, and re-layouts  9.17 us (3%)
  other arithmetic  7.39 us (3%)
    all_gather x1, waiting for transfers between devices, rows_first(): out, at, outs = (lax.all_gather(both, axis, axis=0, tiled=True), 0, [])  133 us
    all_gather x5, blocking collectives, entering(): lax.all_gather(part.astype(kind), axis)  50.5 us
    all_gather x1, waiting for transfers between devices, entering(): lax.all_gather(part.astype(kind), axis)  14.4 us
    all_to_all x2, waiting for transfers between devices, sent_to_all(): return lax.all_to_all(copies, axis, split_axis=0, concat_axis=0, tiled=True)  13.3 us
    all_to_all x1, blocking collectives, sent_and_summed(): lax.all_to_all(blocks, axis, split_axis=0, concat_axis=0, tiled=True)  12.2 us
    all_to_all x2, starting transfers between devices, sent_to_all(): return lax.all_to_all(copies, axis, split_axis=0, concat_axis=0, tiled=True)  8.75 us
    dot_general x5, matrix products, project(): jnp.dot(row_piece, weight, preferred_element_type=jnp.float32)  7.87 us
    ppermute x2, starting transfers between devices, passed_along(): lax.ppermute(value, axis, [(source, source + steps) for source in range(i...  6.78 us
  transfers between devices with their start and end apart: 6, of which 4 were waited for; matrix products, arithmetic and copies ran while one was open for 5% of the time, Pallas kernels for 0%

commit v1 on v0

v1 whole, which is shorter than its diff:
```python
import jax
import jax.numpy as jnp
from jax import lax
from jax.experimental import pallas as pl
from jax.experimental.pallas import tpu as pltpu
from jax.sharding import Mesh
from jax.sharding import PartitionSpec as P

D = 2048
CONV_CH = 1024
CONV_W = 31
BLOCK = 64
ROWS = 16
TOK = 32
CHIP_TOK = 256
Z, X, C, Y = 16, 4, 2, 4
SP = ("sp_0", "sp_1", "sp_2")
SP_TP = ("sp_0", "sp_1", "sp_2", "tp")
MESH = pl.DeviceIdType.MESH
F32 = jnp.float32
BF16 = jnp.bfloat16
HIGH = lax.Precision.HIGHEST

norm_eps = 1e-06
layer_eps = 1e-05

FORGET, INPUT, QUERY, OUTGATE, VALUE, GATE, CONV_OUT, REC_OUT = range(8)


def dot(a, b, dims, precision=None):
    return lax.dot_general(
        a, b, ((dims[:1], dims[1:]), ((), ())), precision=precision, preferred_element_type=F32
    )


def silu(v):
    return v * jax.nn.sigmoid(v)


def kernel(
    tokens, w_forget, w_input, w_query, w_outgate, w_value, w_gate, w_conv_out, w_rec_out,
    gain, taps, cn_gain, cn_bias, margin, jumps, head_gain,
    out,
    W, Xr, Xn, acc, jbuf, jrecv, hsend, hrecv, gext, conv, stat_s, stat_r,
    qt, inner, starts, p1s, p1r, p2s, p2r, p3s, p3r, AO, ps, pr, po, ss, yr,
    local_sem, wd_s, wd_r, ty_s, ty_r, tp_s, tp_r, j_sem, xa_s, xa_r, xb_s, xb_r, z_s, z_r,
    h_sem, st_s, st_r, p1_s, p1_r, p2_s, p2_r, p3_s, p3_r, o_s, o_r, y_s, y_r,
):
    z = lax.axis_index("sp_0")
    x = lax.axis_index("sp_1")
    c = lax.axis_index("sp_2")
    y = lax.axis_index("tp")
    chip = z * X + x
    weights = (w_forget, w_input, w_query, w_outgate, w_value, w_gate, w_conv_out, w_rec_out)
    half = pl.ds(pl.multiple_of(c * 128, 128), 128)
    other_half = pl.ds(pl.multiple_of((1 - c) * 128, 128), 128)

    def at(dz=0, dx=0, dc=0, dy=0):
        return (
            lax.rem(z + (dz + Z), Z), lax.rem(x + (dx + X), X), lax.rem(c + dc, C),
            lax.rem(y + (dy + Y), Y),
        )

    def send(src, dst, s, r, to):
        return pltpu.make_async_remote_copy(src, dst, s, r, device_id=to, device_id_type=MESH)

    partner = at(dc=1)
    nxt = lax.rem(chip + 1, Z * X)
    prv = lax.rem(chip + Z * X - 1, Z * X)
    next_chip = (nxt // X, lax.rem(nxt, X), c, y)
    prev_chip = (prv // X, lax.rem(prv, X), c, y)

    mine = c * Y + y
    own_tokens = pltpu.make_async_copy(tokens, Xr.at[mine], local_sem.at[8])
    own_tokens.start()
    rows = pl.ds(pl.multiple_of(c * ROWS, ROWS), ROWS)
    own_weights = [
        pltpu.make_async_copy(w.at[:, half], W.at[chip, m, rows], local_sem.at[m])
        for m, w in enumerate(weights)
    ]
    for copy in own_weights:
        copy.start()

    barrier = pltpu.get_barrier_semaphore()
    peers = [partner, next_chip, prev_chip]
    peers += [at(dx=d) for d in range(1, X)]
    peers += [at(dy=d) for d in range(1, Y)] + [at(dy=d, dc=1) for d in range(1, Y)]
    peers += [at(dz=d) for d in range(1, Z)]
    for peer in peers:
        pl.semaphore_signal(barrier, inc=1, device_id=peer, device_id_type=MESH)
    for h in range(2):
        jbuf[h] = jnp.broadcast_to(jumps[h : h + 1, :], (8, 128))
    pl.semaphore_wait(barrier, len(peers))

    sends = []
    for m, w in enumerate(weights):
        copy = send(w.at[:, other_half], W.at[chip, m, rows], wd_s.at[m], wd_r.at[m], partner)
        copy.start()
        sends.append(copy)
    for d in range(1, Y):
        copy = send(tokens, Xr.at[mine], ty_s.at[d], ty_r.at[d], at(dy=d))
        copy.start()
        sends.append(copy)
    copy = send(tokens, Xr.at[mine], tp_s.at[0], tp_r.at[0], partner)
    copy.start()
    sends.append(copy)
    jcopy = send(jbuf.at[1 - c], jrecv, j_sem.at[0], j_sem.at[1], partner)
    jcopy.start()
    sends.append(jcopy)

    prows = pl.ds(pl.multiple_of((1 - c) * ROWS, ROWS), ROWS)
    for m, w in enumerate(weights):
        own_weights[m].wait()
        send(w.at[:, half], W.at[chip, m, prows], wd_s.at[m], wd_r.at[m], partner).wait_recv()

    def z_slot(zo, m):
        if m < 2:
            return W.at[pl.ds(zo * X, X), pl.ds(2 * m, 2)]
        return W.at[zo * X + x, pl.ds(4, 4)]

    def z_copy(way, step, m):
        zo = lax.rem(z + Z + (step - 1) * (1 if way else -1), Z)
        return send(
            z_slot(zo, m), z_slot(zo, m), z_s.at[way, step, m], z_r.at[way, step, m],
            at(dz=-1 if way else 1),
        )

    def z_arrival(way, step, m):
        zo = lax.rem(z + Z + step * (1 if way else -1), Z)
        return send(
            z_slot(zo, m), z_slot(zo, m), z_s.at[way, step, m], z_r.at[way, step, m],
            at(dz=-1 if way else 1),
        )

    def xb_copy(zo, d, own=True):
        slot = W.at[zo * X + (x if own else lax.rem(x + X - d, X)), pl.ds(4, 4)]
        return send(slot, slot, xb_s.at[d, zo], xb_r.at[d, zo], at(dx=d))

    for way in range(2):
        z_copy(way, 1, 2).start()
    slot = W.at[chip, pl.ds(0, 4)]
    for d in range(1, X):
        copy = send(slot, slot, xa_s.at[d], xa_r.at[d], at(dx=d))
        copy.start()
        sends.append(copy)
    for d in range(1, X):
        from_x = W.at[z * X + lax.rem(x + X - d, X), pl.ds(0, 4)]
        send(from_x, from_x, xa_s.at[d], xa_r.at[d], at(dx=d)).wait_recv()
    for m in range(2):
        for way in range(2):
            z_copy(way, 1, m).start()
    for d in range(1, X):
        xb_copy(z, d).start()

    for d in range(1, Y):
        slot = Xr.at[c * Y + lax.rem(y + Y - d, Y)]
        send(tokens, slot, ty_s.at[d], ty_r.at[d], at(dy=d)).wait_recv()
        copy = send(slot, slot, tp_s.at[d], tp_r.at[d], partner)
        copy.start()
        sends.append(copy)

    half_way = Z // 2
    furthest = ((half_way, half_way - 1, half_way), (half_way - 1, half_way, half_way - 1))

    def ring_step(step, last):
        for m in (2, 0, 1):
            for way in range(2):
                if last and furthest[way][m] < half_way:
                    continue
                z_arrival(way, step, m).wait_recv()
                if not last:
                    z_copy(way, step + 1, m).start()
                if m == 2:
                    zo = lax.rem(z + Z + step * (1 if way else -1), Z)
                    for d in range(1, X):
                        xb_copy(zo, d).start()

    def inner_step(step, carry):
        ring_step(step, False)
        return carry

    lax.fori_loop(1, half_way - 1, inner_step, 0)
    for m in (2, 0, 1):
        for way in range(2):
            step = half_way - 1
            z_arrival(way, step, m).wait_recv()
            if furthest[way][m] == half_way:
                z_copy(way, half_way, m).start()
            if m == 2:
                zo = lax.rem(z + Z + step * (1 if way else -1), Z)
                for d in range(1, X):
                    xb_copy(zo, d).start()

    own_tokens.wait()
    for d in range(Y):
        slot = Xr.at[(1 - c) * Y + lax.rem(y + Y - d, Y)]
        send(slot, slot, tp_s.at[d], tp_r.at[d], partner).wait_recv()

    def norm_body(i, carry):
        v = Xr[i // 2, pl.ds(pl.multiple_of(lax.rem(i, 2) * 16, 16), 16), :].astype(F32)
        v = v * lax.rsqrt(jnp.mean(v * v, axis=1, keepdims=True) + norm_eps) * gain[...]
        v = v.astype(BF16)
        for k in range(8):
            Xn[k, pl.ds(pl.multiple_of(i * 16, 16), 16), :] = v[:, k * 256 : (k + 1) * 256]
        return carry

    lax.fori_loop(0, CHIP_TOK // 16, norm_body, 0)
    acc[...] = jnp.zeros_like(acc)

    ring_step(half_way, True)

    def x_wait(zo, carry):
        for d in range(1, X):
            xb_copy(zo, d, own=False).wait_recv()
        return carry

    lax.fori_loop(0, Z, x_wait, 0)

    def weight_block(k, m):
        return W[pl.ds(k * 8, 8), m].reshape(256, 128)

    def project(k, carry):
        xk = Xn[k]
        for p in range(3):
            wk = jnp.concatenate([weight_block(k, 2 * p), weight_block(k, 2 * p + 1)], axis=1)
            acc[:, p * 256 : (p + 1) * 256] += dot(xk, wk, (1, 0))
        return carry

    lax.fori_loop(0, 8, project, 0)

    def projected(m, rows):
        return acc[rows, m * 128 : (m + 1) * 128].astype(BF16)

    last_rows = pl.ds(CHIP_TOK - 32, 32)
    hsend[0] = projected(VALUE, last_rows)
    hsend[1] = projected(GATE, last_rows)
    halo = send(hsend, hrecv, h_sem.at[0], h_sem.at[1], next_chip)
    halo.start()
    sends.append(halo)

    jcopy.wait_recv()
    row_at = lax.broadcasted_iota(jnp.int32, (BLOCK, BLOCK), 0)
    col_at = lax.broadcasted_iota(jnp.int32, (BLOCK, BLOCK), 1)
    causal = row_at >= col_at
    lower = causal.astype(F32)
    own_jump = jnp.broadcast_to(jbuf[c][0:1], (128, 128)).T
    far_jump = jnp.broadcast_to(jrecv[0:1], (128, 128)).T
    first = c == 0
    jump_of = (jnp.where(first, own_jump, far_jump), jnp.where(first, far_jump, own_jump))
    mar = margin[:, half]
    state = jnp.zeros((128, 128), F32)
    total = jnp.zeros((1, 128), F32)
    before = []
    for b in range(CHIP_TOK // BLOCK):
        blk = slice(b * BLOCK, (b + 1) * BLOCK)
        f = projected(FORGET, blk).astype(F32)
        v = projected(INPUT, blk)
        q = silu(projected(QUERY, blk).astype(F32))
        key = mar * jax.nn.sigmoid(-f)
        kept = 1.0 - key
        log_forget = jnp.where(kept == 1.0, -key, jnp.log(kept) * (key / (1.0 - kept)))
        jb = jump_of[b // 2][(b % 2) * BLOCK : (b % 2 + 1) * BLOCK]
        cum = dot(lower, log_forget + jb, (1, 0), HIGH)
        fin = cum[BLOCK - 1 : BLOCK, :]
        q_t = (q * jnp.exp(cum)).astype(BF16)
        k_t = (key * jnp.exp(-cum)).astype(BF16)
        k_f = (key * jnp.exp(fin - cum)).astype(BF16)
        scores = jnp.where(causal, dot(q_t, k_t, (1, 1)), 0.0).astype(BF16)
        inner[blk, :] = dot(scores, v, (1, 0))
        qt[blk, :] = q_t
        starts[b] = state
        before.append(total)
        state = jnp.exp(fin) * state + dot(v, k_f, (0, 0))
        total = total + fin

    upper8 = lax.broadcasted_iota(jnp.int32, (16, 128), 0) < 8

    def pack_decay(a):
        hi = a.astype(BF16).astype(F32)
        return jnp.where(upper8, hi, a - hi).astype(BF16)

    def unpack_decay(block):
        block = block.astype(F32)
        return block[0:1] + block[8:9]

    decay_rows = pack_decay(total)
    for j in range(X):
        p1s[j, 0:32, :] = state[32 * j : 32 * (j + 1)].astype(BF16)
        p1s[j, 32:48, :] = decay_rows
    for d in range(1, X):
        j = lax.rem(x + d, X)
        copy = send(p1s.at[j], p1r.at[x], p1_s.at[d], p1_r.at[d], at(dx=d))
        copy.start()
        sends.append(copy)

    halo.wait_recv()
    halo_rows = hrecv[0].astype(F32) * jax.nn.sigmoid(hrecv[1].astype(F32))
    gext[0:32, :] = jnp.where(chip == 0, 0.0, halo_rows)
    for b in range(CHIP_TOK // BLOCK):
        blk = slice(b * BLOCK, (b + 1) * BLOCK)
        gext[32 + b * BLOCK : 32 + (b + 1) * BLOCK, :] = projected(VALUE, blk).astype(
            F32
        ) * jax.nn.sigmoid(projected(GATE, blk).astype(F32))
    tap_rows = taps[:, half]
    for b in range(CHIP_TOK // BLOCK):
        base = gext[b * BLOCK : b * BLOCK + BLOCK + 32, :]
        total_c = jnp.zeros((BLOCK, 128), F32)
        for j in range(CONV_W):
            total_c += tap_rows[j : j + 1] * base[2 + j : 2 + j + BLOCK]
        conv[b * BLOCK : (b + 1) * BLOCK, :] = total_c.astype(BF16).astype(F32)
    top = lax.broadcasted_iota(jnp.int32, (8, 128), 0) < 4
    for h in range(2):
        turned = conv[h * 128 : (h + 1) * 128, :].T
        first_sum = jnp.sum(turned, axis=0, keepdims=True)
        second_sum = jnp.sum(turned * turned, axis=0, keepdims=True)
        stat_s[:, h * 128 : (h + 1) * 128] = jnp.where(top, first_sum, second_sum)
    for dc in range(C):
        for d in range(Y):
            if dc + d:
                i = dc * Y + d
                copy = send(stat_s, stat_r.at[i], st_s.at[i], st_r.at[i], at(dc=dc, dy=d))
                copy.start()
                sends.append(copy)

    for d in range(1, X):
        j = lax.rem(x + X - d, X)
        send(p1s.at[j], p1r.at[j], p1_s.at[d], p1_r.at[d], at(dx=d)).wait_recv()
    p1r[x] = p1s[x]
    state_in = jnp.zeros((32, 128), F32)
    decay_in = jnp.zeros((1, 128), F32)
    ahead = []
    for j in range(X):
        ahead.append((state_in, decay_in))
        a = unpack_decay(p1r[j, 32:48, :])
        state_in = jnp.exp(a) * state_in + p1r[j, 0:32, :].astype(F32)
        decay_in = decay_in + a
    p2s[0:32, :] = state_in.astype(BF16)
    p2s[32:48, :] = pack_decay(decay_in)
    for d in range(1, Z):
        copy = send(p2s, p2r.at[z], p2_s.at[d], p2_r.at[d], at(dz=d))
        copy.start()
        sends.append(copy)

    for dc in range(C):
        for d in range(Y):
            if dc + d:
                i = dc * Y + d
                send(stat_s, stat_r.at[i], st_s.at[i], st_r.at[i], partner).wait_recv()
    sums = stat_s[...]
    for i in range(1, C * Y):
        sums = sums + stat_r[i]
    for h in range(2):
        blk = slice(h * 128, (h + 1) * 128)
        mean = jnp.broadcast_to(sums[0:1, blk], (128, 128)).T / CONV_CH
        square = jnp.broadcast_to(sums[4:5, blk], (128, 128)).T / CONV_CH
        shifted = (conv[blk, :] - mean) * lax.rsqrt(square - mean * mean + layer_eps)
        AO[blk, 0:128] = silu(shifted * cn_gain[:, half] + cn_bias[:, half]).astype(BF16)

    for d in range(1, Z):
        zo = lax.rem(z + Z - d, Z)
        send(p2s, p2r.at[zo], p2_s.at[d], p2_r.at[d], at(dz=d)).wait_recv()

    def over_z(zo, carried):
        a = unpack_decay(p2r[zo, 32:48, :])
        return jnp.exp(a) * carried + p2r[zo, 0:32, :].astype(F32)

    carried = lax.fori_loop(0, z, over_z, jnp.zeros((32, 128), F32))
    for j in range(X):
        p3s[j] = (jnp.exp(ahead[j][1]) * carried + ahead[j][0]).astype(BF16)
    for d in range(1, X):
        j = lax.rem(x + d, X)
        copy = send(p3s.at[j], p3r.at[x], p3_s.at[d], p3_r.at[d], at(dx=d))
        copy.start()
        sends.append(copy)
    for d in range(1, X):
        j = lax.rem(x + X - d, X)
        send(p3s.at[j], p3r.at[j], p3_s.at[d], p3_r.at[d], at(dx=d)).wait_recv()
    p3r[x] = p3s[x]
    incoming = p3r[...].astype(F32).reshape(128, 128)
    for b in range(CHIP_TOK // BLOCK):
        blk = slice(b * BLOCK, (b + 1) * BLOCK)
        start = (starts[b] + jnp.exp(before[b]) * incoming).astype(BF16)
        rec = inner[blk, :] + dot(qt[blk, :], start, (1, 1))
        rec = rec * lax.rsqrt(jnp.mean(rec * rec, axis=1, keepdims=True) + norm_eps)
        rec = rec * head_gain[:, half] * silu(projected(OUTGATE, blk).astype(F32))
        AO[blk, 128:256] = rec.astype(BF16)

    keep = pl.ds(pl.multiple_of(c * 128, 128), 128)
    give = pl.ds(pl.multiple_of((1 - c) * 128, 128), 128)

    def out_copy(n):
        return send(ps.at[n], pr.at[n], o_s.at[n], o_r.at[n], partner)

    def out_body(n, carry):
        wn = jnp.concatenate([weight_block(n, CONV_OUT), weight_block(n, REC_OUT)], axis=1)
        ps[n] = dot(AO[give, :], wn, (1, 1)).astype(BF16)
        po[n] = dot(AO[keep, :], wn, (1, 1))
        out_copy(n).start()
        return carry

    lax.fori_loop(0, 8, out_body, 0)

    def y_copy(g, d):
        part = pl.ds(g * 2, 2)
        j = lax.rem(y + d, Y)
        return send(
            ss.at[part, j], yr.at[d, part], y_s.at[d, g], y_r.at[d, g], at(dy=d)
        )

    for g in range(4):
        for n in (2 * g, 2 * g + 1):
            out_copy(n).wait_recv()
            summed = po[n] + pr[n].astype(F32)
            ss[n] = summed.astype(BF16).reshape(Y, TOK, 256)
        for d in range(1, Y):
            y_copy(g, d).start()
    for g in range(4):
        for d in range(1, Y):
            y_copy(g, d).wait_recv()
        for n in (2 * g, 2 * g + 1):
            mixed = ss[n, y].astype(F32)
            for d in range(1, Y):
                mixed = mixed + yr[d, n].astype(F32)
            out[:, n * 256 : (n + 1) * 256] = mixed.astype(BF16)

    for copy in sends:
        copy.wait_send()

    def z_drain(step, carry):
        for way in range(2):
            for m in range(3):
                z_copy(way, step, m).wait_send()
        return carry

    lax.fori_loop(1, half_way, z_drain, 0)
    for way in range(2):
        for m in range(3):
            if furthest[way][m] == half_way:
                z_copy(way, half_way, m).wait_send()

    def x_drain(zo, carry):
        for d in range(1, X):
            xb_copy(zo, d).wait_send()
        return carry

    lax.fori_loop(0, Z, x_drain, 0)
    for n in range(8):
        out_copy(n).wait_send()
    for g in range(4):
        for d in range(1, Y):
            y_copy(g, d).wait_send()


def per_device(
    tokens,
    input_norm_gain,
    convolution_value_weight,
    convolution_gate_weight,
    depthwise_filter_taps,
    channel_norm_gain,
    channel_norm_bias,
    query_projection_weight,
    forget_gate_weight,
    recurrence_value_weight,
    output_gate_weight,
    forget_floor_margin,
    decay_jump_terms,
    head_norm_gain,
    convolution_output_weight,
    recurrence_output_weight,
):
    hbm = pl.BlockSpec(memory_space=pl.ANY)
    vmem = pl.BlockSpec(memory_space=pltpu.VMEM)
    dma = pltpu.SemaphoreType.DMA
    chips = Z * X
    return pl.pallas_call(
        kernel,
        name="layer",
        out_shape=jax.ShapeDtypeStruct((TOK, D), BF16),
        in_specs=[hbm] * 9 + [vmem] * 7,
        out_specs=vmem,
        scratch_shapes=[
            pltpu.VMEM((chips, 8, 2 * ROWS, 128), BF16),
            pltpu.VMEM((C * Y, TOK, D), BF16),
            pltpu.VMEM((8, CHIP_TOK, 256), BF16),
            pltpu.VMEM((CHIP_TOK, 768), F32),
            pltpu.VMEM((2, 8, 128), F32),
            pltpu.VMEM((8, 128), F32),
            pltpu.VMEM((2, 32, 128), BF16),
            pltpu.VMEM((2, 32, 128), BF16),
            pltpu.VMEM((32 + CHIP_TOK, 128), F32),
            pltpu.VMEM((CHIP_TOK, 128), F32),
            pltpu.VMEM((8, CHIP_TOK), F32),
            pltpu.VMEM((C * Y, 8, CHIP_TOK), F32),
            pltpu.VMEM((CHIP_TOK, 128), BF16),
            pltpu.VMEM((CHIP_TOK, 128), F32),
            pltpu.VMEM((4, 128, 128), F32),
            pltpu.VMEM((X, 48, 128), BF16),
            pltpu.VMEM((X, 48, 128), BF16),
            pltpu.VMEM((48, 128), BF16),
            pltpu.VMEM((Z, 48, 128), BF16),
            pltpu.VMEM((X, 32, 128), BF16),
            pltpu.VMEM((X, 32, 128), BF16),
            pltpu.VMEM((CHIP_TOK, 256), BF16),
            pltpu.VMEM((8, 128, 256), BF16),
            pltpu.VMEM((8, 128, 256), BF16),
            pltpu.VMEM((8, 128, 256), F32),
            pltpu.VMEM((8, Y, TOK, 256), BF16),
            pltpu.VMEM((Y, 8, TOK, 256), BF16),
            dma((9,)),
            dma((8,)), dma((8,)),
            dma((Y,)), dma((Y,)),
            dma((Y,)), dma((Y,)),
            dma((2,)),
            dma((X,)), dma((X,)),
            dma((X, Z)), dma((X, Z)),
            dma((2, Z // 2 + 1, 3)), dma((2, Z // 2 + 1, 3)),
            dma((2,)),
            dma((C * Y,)), dma((C * Y,)),
            dma((X,)), dma((X,)),
            dma((Z,)), dma((Z,)),
            dma((X,)), dma((X,)),
            dma((8,)), dma((8,)),
            dma((Y, 4)), dma((Y, 4)),
        ],
        compiler_params=pltpu.CompilerParams(
            collective_id=0, has_side_effects=True, vmem_limit_bytes=56 * 1024 * 1024
        ),
    )(
        tokens,
        forget_gate_weight,
        recurrence_value_weight,
        query_projection_weight,
        output_gate_weight,
        convolution_value_weight,
        convolution_gate_weight,
        convolution_output_weight.T,
        recurrence_output_weight.T,
        input_norm_gain[None],
        depthwise_filter_taps,
        channel_norm_gain[None],
        channel_norm_bias[None],
        forget_floor_margin[None],
        decay_jump_terms,
        head_norm_gain[None],
    )


def solution(mesh):
    split = Mesh(mesh.devices.reshape(Z, X, C, Y), SP_TP)
    return jax.shard_map(
        per_device,
        mesh=split,
        in_specs=(
            P(SP_TP, None),
            P(),
            P(SP, "tp"),
            P(SP, "tp"),
            P(None, "tp"),
            P("tp"),
            P("tp"),
            P(SP, "tp"),
            P(SP, "tp"),
            P(SP, "tp"),
            P(SP, "tp"),
            P("tp"),
            P("tp", SP),
            P("tp"),
            P("tp", SP),
            P("tp", SP),
        ),
        out_specs=P(SP_TP, None),
        check_vma=False,
    )
```

time: 285 us -> 96.3 us (0.34)
  the two profiles are of different devices: /device:TPU:6 before, /device:TPU:4 now
where the time goes in v1:
time: 96.3 us; the launch traced here: 96.1 us
  Pallas kernels  94.6 us (98%)
  local copies, waits for them, and re-layouts  1.57 us (2%)
    pallas_call x1, Pallas kernels, per_device(): pl.pallas_call(kernel, name='layer', out_shape=jax.ShapeDtypeStruct((TOK,...  94.6 us

profile of v1, /device:TPU:4, one launch (start us, length us, event | category | flops | bytes accessed | tf_op | source)
XLA Modules:
  0.0 96.1 jit_solution(1980375927026864294)
XLA Ops:
  0.0 94.6 %layer.1 = bf16[32,2048]{1,0:T(8,128)(2,1)} custom-call(bf16[32,2048]{1,0:T(8,128)(2,1)} %tokens.1, bf16[16,256]{1,0:T(8,128)(2,1)} %w_forget.1, bf16[16,256]{1,0:T(8,128)(2,1)} %w_input.1, bf16[16,256]{1,0:T(8,128)(2,1)} %w_query.1, bf16[16,256]{1,0:T(8,128)(2,1)} %w_outgate.1, bf16[16,256]{1,0:T(8,128)(2,1)} %w_value.1, bf16[16,256]{1,0:T(8,128)(2,1)} %w_gate.1, ...), custom_call_target="tpu_custom_call" | custom-call | tf_op jit(solution)/shard_map/layer/pallas_call | solution.py:476
  94.6 1.6 %copy.18 = bf16[32,2048]{1,0:T(8,128)(2,1)} copy(bf16[32,2048]{1,0:T(8,128)(2,1)} %layer.1) | data formatting | bytes 262144

commit v2 on v1

v2 whole, which is shorter than its diff:
```python
import jax
import jax.numpy as jnp
from jax import lax
from jax.experimental import pallas as pl
from jax.experimental.pallas import tpu as pltpu
from jax.sharding import Mesh
from jax.sharding import PartitionSpec as P

D = 2048
CONV_CH = 1024
CONV_W = 31
BLOCK = 64
ROWS = 16
TOK = 32
CHIP_TOK = 256
Z, X, C, Y = 16, 4, 2, 4
SP = ("sp_0", "sp_1", "sp_2")
SP_TP = ("sp_0", "sp_1", "sp_2", "tp")
MESH = pl.DeviceIdType.MESH
F32 = jnp.float32
BF16 = jnp.bfloat16
HIGH = lax.Precision.HIGHEST

norm_eps = 1e-06
layer_eps = 1e-05

FORGET, INPUT, OUTGATE, QUERY, VALUE, GATE, CONV_OUT, REC_OUT = range(8)


def dot(a, b, dims, precision=None):
    return lax.dot_general(
        a, b, ((dims[:1], dims[1:]), ((), ())), precision=precision, preferred_element_type=F32
    )


def silu(v):
    return v * jax.nn.sigmoid(v)


def kernel(
    tokens, w_forget, w_input, w_outgate, w_query, w_value, w_gate, w_conv_out, w_rec_out,
    gain_in, taps_in, cn_gain_in, cn_bias_in, margin_in, jumps_in, head_gain_in,
    out,
    W, Xr, Xn, accs, acc, gain, taps, cn_gain, cn_bias, margin, jumps, head_gain,
    jbuf, jrecv, hsend, hrecv, gext, conv, stat_s, stat_r, keys, cums, qt, inner, starts,
    p1s, p1r, p2s, p2r, p3s, p3r, AO, ps, pr, ss, yr, ob,
    local_sem, one_s, z_s, one_r, ty_r, z_r, xb_r, o_r, y_r,
):
    z = lax.axis_index("sp_0")
    x = lax.axis_index("sp_1")
    c = lax.axis_index("sp_2")
    y = lax.axis_index("tp")
    chip = z * X + x
    weights = (w_forget, w_input, w_outgate, w_query, w_value, w_gate, w_conv_out, w_rec_out)
    half = pl.ds(pl.multiple_of(c * 128, 128), 128)
    other_half = pl.ds(pl.multiple_of((1 - c) * 128, 128), 128)

    def at(dz=0, dx=0, dc=0, dy=0):
        return (
            lax.rem(z + (dz + Z), Z), lax.rem(x + (dx + X), X), lax.rem(c + dc, C),
            lax.rem(y + (dy + Y), Y),
        )

    def send(src, dst, s, r, to):
        return pltpu.make_async_remote_copy(src, dst, s, r, device_id=to, device_id_type=MESH)

    partner = at(dc=1)

    def arrived(ref, r):
        send(ref, ref, one_s.at[0], r, partner).wait_recv()

    def left(ref, s):
        send(ref, ref, s, one_r.at[0], partner).wait_send()

    nxt = lax.rem(chip + 1, Z * X)
    prv = lax.rem(chip + Z * X - 1, Z * X)
    next_chip = (nxt // X, lax.rem(nxt, X), c, y)
    prev_chip = (prv // X, lax.rem(prv, X), c, y)

    mine = c * Y + y
    own_tokens = pltpu.make_async_copy(tokens, Xr.at[mine], local_sem.at[0])
    rows = pl.ds(pl.multiple_of(c * ROWS, ROWS), ROWS)
    for m, w in enumerate(weights):
        pltpu.make_async_copy(w.at[:, half], W.at[chip, m, rows], local_sem.at[1]).start()
    own_tokens.start()
    small = ((gain_in, gain), (taps_in, taps), (cn_gain_in, cn_gain), (cn_bias_in, cn_bias),
             (margin_in, margin), (head_gain_in, head_gain), (jumps_in, jumps))
    small = [pltpu.make_async_copy(a, b, local_sem.at[2 + i]) for i, (a, b) in enumerate(small)]
    for copy in small:
        copy.start()

    barrier = pltpu.get_barrier_semaphore()
    peers = [partner, next_chip, prev_chip]
    peers += [at(dx=d) for d in range(1, X)]
    peers += [at(dy=d) for d in range(1, Y)] + [at(dy=d, dc=1) for d in range(1, Y)]
    peers += [at(dz=d) for d in range(1, Z)]
    for peer in peers:
        pl.semaphore_signal(barrier, inc=1, device_id=peer, device_id_type=MESH)
    pl.semaphore_wait(barrier, len(peers))

    for m, w in enumerate(weights):
        send(w.at[:, other_half], W.at[chip, m, rows], one_s.at[0], one_r.at[0], partner).start()
    for d in range(1, Y):
        send(tokens, Xr.at[mine], one_s.at[1], ty_r.at[d], at(dy=d)).start()
    send(tokens, Xr.at[mine], one_s.at[2], one_r.at[1], partner).start()
    own_rows = W.at[chip, :, rows]
    pltpu.make_async_copy(own_rows, own_rows, local_sem.at[1]).wait()
    arrived(W.at[chip, pl.ds(0, 4)], one_r.at[0])

    def z_slot(zo, m):
        if m == 2:
            return W.at[zo * X + x, pl.ds(3, 5)]
        return W.at[pl.ds(zo * X, X), pl.ds(0, 2) if m == 0 else pl.ds(2, 1)]

    def z_row(way, step):
        return lax.rem(z + Z + step * (1 if way else -1), Z)

    def z_copy(way, step, m, zo):
        return send(
            z_slot(zo, m), z_slot(zo, m), z_s.at[m], z_r.at[way, step, m], at(dz=-1 if way else 1)
        )

    def z_send(way, step, m):
        z_copy(way, step, m, z_row(way, step - 1)).start()

    def z_wait(way, step, m):
        z_copy(way, step, m, z_row(way, step)).wait_recv()

    def x_slot(zo, dx):
        return W.at[zo * X + lax.rem(x + X + dx, X), pl.ds(3, 5)]

    def x_half(zo, dx, side):
        return W.at[zo * X + lax.rem(x + X + dx, X), pl.ds(3, 5), pl.ds(side * 16, 16)]

    def x_send(zo):
        for side, dx in ((0, 1), (1, -1)):
            slot = x_slot(zo, 0)
            send(slot, slot, one_s.at[3], xb_r.at[side, zo], at(dx=dx)).start()

    def x_forward(zo):
        for side, dx in ((0, 1), (1, -1)):
            arrived(x_slot(zo, -dx), xb_r.at[side, zo])
            part = x_half(zo, -dx, side)
            send(part, part, one_s.at[4], one_r.at[2], at(dx=dx)).start()

    for way in range(2):
        z_send(way, 1, 2)
    slot = W.at[chip, pl.ds(0, 3)]
    for d in range(1, X):
        send(slot, slot, one_s.at[5], one_r.at[3], at(dx=d)).start()
    x_send(z)
    arrived(W.at[pl.ds(0, 3), pl.ds(0, 3)], one_r.at[3])
    for m in range(2):
        for way in range(2):
            z_send(way, 1, m)

    def row_block(zo, m):
        return W[pl.ds(zo * X, X), m].reshape(128, 128)

    def project_rows(za, zb, first):
        xk = jnp.concatenate([Xn[za], Xn[zb]], axis=1)
        wk = jnp.concatenate(
            [
                jnp.concatenate([row_block(za, m), row_block(zb, m)], axis=0)
                for m in (FORGET, INPUT)
            ],
            axis=1,
        )
        part = dot(xk, wk, (1, 0))
        accs[...] = part if first else accs[...] + part

    half_way = Z // 2
    furthest = ((half_way, half_way - 1, half_way - 1), (half_way - 1, half_way, half_way))
    for step in range(1, half_way):
        for m in (0, 2, 1):
            for way in range(2):
                z_wait(way, step, m)
                if furthest[way][m] > step:
                    z_send(way, step + 1, m)
                if m == 2:
                    x_send(z_row(way, step))
        for way in range(2):
            if way == 0 or step > 1:
                x_forward(z_row(way, step - 1))
        if step == 1:
            for d in range(1, Y):
                slot = Xr.at[c * Y + lax.rem(y + Y - d, Y)]
                arrived(slot, ty_r.at[d])
                send(slot, slot, one_s.at[2], one_r.at[1], partner).start()
            for h in range(2):
                if h == 0:
                    small[6].wait()
                jbuf[h] = jnp.broadcast_to(jumps[h : h + 1, :], (8, 128))
        if step == 2:
            send(jbuf.at[1 - c], jrecv, one_s.at[6], one_r.at[4], partner).start()
            own_tokens.wait()
            small[0].wait()
            arrived(Xr.at[pl.ds(0, 4)], one_r.at[1])

            def norm_body(i, carry):
                at_row = pl.multiple_of(lax.rem(i, 2) * 16, 16)
                v = Xr[i // 2, pl.ds(at_row, 16), :].astype(F32)
                v = v * lax.rsqrt(jnp.mean(v * v, axis=1, keepdims=True) + norm_eps) * gain[...]
                v = v.astype(BF16)
                for k in range(Z):
                    Xn[k, pl.ds(pl.multiple_of(i * 16, 16), 16), :] = v[:, k * 128 : (k + 1) * 128]
                return carry

            lax.fori_loop(0, CHIP_TOK // 16, norm_body, 0)
        if step >= 3:
            for s in (step, step - 2) if step < 5 else (step,):
                project_rows(z_row(0, s), z_row(1, s), s == 3)

    z_wait(0, half_way, 0)
    z_wait(1, half_way, 2)
    far = z_row(0, half_way)
    x_send(far)
    for way in range(2):
        x_forward(z_row(way, half_way - 1))
    project_rows(z, far, False)

    arrived(jrecv, one_r.at[4])
    for copy in small[1:6]:
        copy.wait()
    row_at = lax.broadcasted_iota(jnp.int32, (BLOCK, BLOCK), 0)
    col_at = lax.broadcasted_iota(jnp.int32, (BLOCK, BLOCK), 1)
    causal = row_at >= col_at
    lower = causal.astype(F32)
    own_jump = jnp.broadcast_to(jbuf[c][0:1], (128, 128)).T
    far_jump = jnp.broadcast_to(jrecv[0:1], (128, 128)).T
    first = c == 0
    jump_of = (jnp.where(first, own_jump, far_jump), jnp.where(first, far_jump, own_jump))
    mar = margin[:, half]
    blocks = [slice(b * BLOCK, (b + 1) * BLOCK) for b in range(CHIP_TOK // BLOCK)]
    state = jnp.zeros((128, 128), F32)
    total = jnp.zeros((1, 128), F32)
    before = []
    for b, blk in enumerate(blocks):
        f = accs[blk, 0:128].astype(BF16).astype(F32)
        v = accs[blk, 128:256].astype(BF16)
        key = mar * jax.nn.sigmoid(-f)
        kept = 1.0 - key
        log_forget = jnp.where(kept == 1.0, -key, jnp.log(kept) * (key / (1.0 - kept)))
        jb = jump_of[b // 2][(b % 2) * BLOCK : (b % 2 + 1) * BLOCK]
        cum = dot(lower, log_forget + jb, (1, 0), HIGH)
        fin = cum[BLOCK - 1 : BLOCK, :]
        k_f = (key * jnp.exp(fin - cum)).astype(BF16)
        keys[blk, :] = key
        cums[blk, :] = cum
        starts[b] = state
        before.append(total)
        state = jnp.exp(fin) * state + dot(v, k_f, (0, 0))
        total = total + fin

    upper8 = lax.broadcasted_iota(jnp.int32, (16, 128), 0) < 8

    def pack_decay(a):
        hi = a.astype(BF16).astype(F32)
        return jnp.where(upper8, hi, a - hi).astype(BF16)

    def unpack_decay(block):
        block = block.astype(F32)
        return block[0:1] + block[8:9]

    decay_rows = pack_decay(total)
    for j in range(X):
        p1s[j, 0:32, :] = state[32 * j : 32 * (j + 1)].astype(BF16)
        p1s[j, 32:48, :] = decay_rows
    for d in range(1, X):
        send(p1s.at[lax.rem(x + d, X)], p1r.at[x], one_s.at[7], one_r.at[5], at(dx=d)).start()
    x_forward(far)
    p1r[x] = p1s[x]
    arrived(p1s.at[pl.ds(0, X - 1)], one_r.at[5])
    state_in = jnp.zeros((32, 128), F32)
    decay_in = jnp.zeros((1, 128), F32)
    ahead = []
    for j in range(X):
        ahead.append((state_in, decay_in))
        a = unpack_decay(p1r[j, 32:48, :])
        state_in = jnp.exp(a) * state_in + p1r[j, 0:32, :].astype(F32)
        decay_in = decay_in + a
    p2s[0:32, :] = state_in.astype(BF16)
    p2s[32:48, :] = pack_decay(decay_in)
    for d in range(1, Z):
        send(p2s, p2r.at[z], one_s.at[8], one_r.at[6], at(dz=d)).start()

    z_wait(1, half_way, 1)
    arrived(W.at[pl.ds(0, 10)], one_r.at[2])

    def weight_block(k, m):
        return W[pl.ds(k * 8, 8), m].reshape(256, 128)

    acc[...] = jnp.zeros_like(acc)

    def project(k, carry):
        xk = jnp.concatenate([Xn[2 * k], Xn[2 * k + 1]], axis=1)
        for p in range(2):
            wk = jnp.concatenate(
                [weight_block(k, 2 + 2 * p), weight_block(k, 3 + 2 * p)], axis=1
            )
            acc[:, p * 256 : (p + 1) * 256] += dot(xk, wk, (1, 0))
        return carry

    lax.fori_loop(0, 8, project, 0)

    def projected(m, rows):
        return acc[rows, (m - 2) * 128 : (m - 1) * 128].astype(BF16)

    last_rows = pl.ds(CHIP_TOK - 32, 32)
    hsend[0] = projected(VALUE, last_rows)
    hsend[1] = projected(GATE, last_rows)
    halo = send(hsend, hrecv, one_s.at[9], one_r.at[7], next_chip)
    halo.start()

    for blk in blocks:
        q = silu(projected(QUERY, blk).astype(F32))
        cum = cums[blk, :]
        q_t = (q * jnp.exp(cum)).astype(BF16)
        k_t = (keys[blk, :] * jnp.exp(-cum)).astype(BF16)
        scores = jnp.where(causal, dot(q_t, k_t, (1, 1)), 0.0).astype(BF16)
        inner[blk, :] = dot(scores, accs[blk, 128:256].astype(BF16), (1, 0))
        qt[blk, :] = q_t

    for blk in blocks:
        gext[32 + blk.start : 32 + blk.stop, :] = projected(VALUE, blk).astype(
            F32
        ) * jax.nn.sigmoid(projected(GATE, blk).astype(F32))
    halo.wait_recv()
    halo_rows = hrecv[0].astype(F32) * jax.nn.sigmoid(hrecv[1].astype(F32))
    gext[0:32, :] = jnp.where(chip == 0, 0.0, halo_rows)
    tap_rows = taps[:, half]
    for b, blk in enumerate(blocks):
        base = gext[b * BLOCK : b * BLOCK + BLOCK + 32, :]
        total_c = jnp.zeros((BLOCK, 128), F32)
        for j in range(CONV_W):
            total_c += tap_rows[j : j + 1] * base[2 + j : 2 + j + BLOCK]
        conv[blk, :] = total_c.astype(BF16).astype(F32)
    top = lax.broadcasted_iota(jnp.int32, (8, 128), 0) < 4
    for h in range(2):
        turned = conv[h * 128 : (h + 1) * 128, :].T
        first_sum = jnp.sum(turned, axis=0, keepdims=True)
        second_sum = jnp.sum(turned * turned, axis=0, keepdims=True)
        stat_s[:, h * 128 : (h + 1) * 128] = jnp.where(top, first_sum, second_sum)
    for dc in range(C):
        for d in range(Y):
            if dc + d:
                i = dc * Y + d
                send(
                    stat_s, stat_r.at[i - 1], one_s.at[10], one_r.at[8], at(dc=dc, dy=d)
                ).start()

    arrived(p2r.at[pl.ds(0, Z - 1)], one_r.at[6])

    def over_z(zo, carried):
        a = unpack_decay(p2r[zo, 32:48, :])
        return jnp.exp(a) * carried + p2r[zo, 0:32, :].astype(F32)

    carried = lax.fori_loop(0, z, over_z, jnp.zeros((32, 128), F32))
    for j in range(X):
        p3s[j] = (jnp.exp(ahead[j][1]) * carried + ahead[j][0]).astype(BF16)
    for d in range(1, X):
        send(p3s.at[lax.rem(x + d, X)], p3r.at[x], one_s.at[11], one_r.at[9], at(dx=d)).start()

    arrived(stat_r.at[pl.ds(0, C * Y - 1)], one_r.at[8])
    sums = stat_s[...]
    for i in range(C * Y - 1):
        sums = sums + stat_r[i]
    for h in range(2):
        blk = slice(h * 128, (h + 1) * 128)
        mean = jnp.broadcast_to(sums[0:1, blk], (128, 128)).T / CONV_CH
        square = jnp.broadcast_to(sums[4:5, blk], (128, 128)).T / CONV_CH
        shifted = (conv[blk, :] - mean) * lax.rsqrt(square - mean * mean + layer_eps)
        AO[blk, 0:128] = silu(shifted * cn_gain[:, half] + cn_bias[:, half]).astype(BF16)

    p3r[x] = p3s[x]
    arrived(p3s.at[pl.ds(0, X - 1)], one_r.at[9])
    incoming = p3r[...].astype(F32).reshape(128, 128)
    for b, blk in enumerate(blocks):
        start = (starts[b] + jnp.exp(before[b]) * incoming).astype(BF16)
        rec = inner[blk, :] + dot(qt[blk, :], start, (1, 1))
        rec = rec * lax.rsqrt(jnp.mean(rec * rec, axis=1, keepdims=True) + norm_eps)
        rec = rec * head_gain[:, half] * silu(projected(OUTGATE, blk).astype(F32))
        AO[blk, 128:256] = rec.astype(BF16)

    keep = pl.ds(pl.multiple_of(c * 128, 128), 128)
    give = pl.ds(pl.multiple_of((1 - c) * 128, 128), 128)

    def out_weight(n):
        return jnp.concatenate([weight_block(n, CONV_OUT), weight_block(n, REC_OUT)], axis=1)

    def out_copy(n):
        return send(ps.at[n], pr.at[n], one_s.at[12], o_r.at[n], partner)

    def give_body(n, carry):
        ps[n] = dot(AO[give, :], out_weight(n), (1, 1)).astype(BF16)
        out_copy(n).start()
        return carry

    lax.fori_loop(0, 8, give_body, 0)

    def y_copy(g, d):
        part = pl.ds(g * 2, 2)
        return send(
            ss.at[part, lax.rem(y + d, Y)], yr.at[d - 1, part], one_s.at[13], y_r.at[g], at(dy=d)
        )

    def keep_body(g, carry):
        for i in range(2):
            n = 2 * g + i
            kept_part = dot(AO[keep, :], out_weight(n), (1, 1))
            out_copy(n).wait_recv()
            ss[n] = (kept_part + pr[n].astype(F32)).astype(BF16).reshape(Y, TOK, 256)
        for d in (2, 1, 3):
            y_copy(g, d).start()
        return carry

    lax.fori_loop(0, 4, keep_body, 0)

    for g in range(4):
        arrived(yr.at[pl.ds(0, Y - 1), pl.ds(g * 2, 2)], y_r.at[g])
        for n in (2 * g, 2 * g + 1):
            mixed = ss[n, y].astype(F32)
            for d in range(Y - 1):
                mixed = mixed + yr[d, n].astype(F32)
            ob[:, n * 256 : (n + 1) * 256] = mixed.astype(BF16)
        cols = pl.ds(g * 512, 512)
        pltpu.make_async_copy(ob.at[:, cols], out.at[:, cols], local_sem.at[9]).start()

    left(W.at[0, pl.ds(0, 4)], one_s.at[0])
    left(Xr.at[pl.ds(0, 3)], one_s.at[1])
    left(Xr.at[pl.ds(0, 4)], one_s.at[2])
    left(W.at[pl.ds(0, 20)], one_s.at[3])
    left(W.at[pl.ds(0, 10)], one_s.at[4])
    left(W.at[pl.ds(0, 3), pl.ds(0, 3)], one_s.at[5])
    left(jrecv, one_s.at[6])
    left(p1s.at[pl.ds(0, X - 1)], one_s.at[7])
    left(p2r.at[pl.ds(0, Z - 1)], one_s.at[8])
    left(hsend, one_s.at[9])
    left(stat_r.at[pl.ds(0, C * Y - 1)], one_s.at[10])
    left(p3s.at[pl.ds(0, X - 1)], one_s.at[11])
    left(ps, one_s.at[12])
    left(ss.at[pl.ds(0, 6)], one_s.at[13])
    left(W.at[pl.ds(0, 15)], z_s.at[0])
    left(W.at[pl.ds(0, 15), pl.ds(0, 4)], z_s.at[1])
    left(W.at[pl.ds(0, 15), pl.ds(0, 5)], z_s.at[2])
    pltpu.make_async_copy(ob, out, local_sem.at[9]).wait()


def per_device(
    tokens,
    input_norm_gain,
    convolution_value_weight,
    convolution_gate_weight,
    depthwise_filter_taps,
    channel_norm_gain,
    channel_norm_bias,
    query_projection_weight,
    forget_gate_weight,
    recurrence_value_weight,
    output_gate_weight,
    forget_floor_margin,
    decay_jump_terms,
    head_norm_gain,
    convolution_output_weight,
    recurrence_output_weight,
):
    hbm = pl.BlockSpec(memory_space=pl.ANY)
    dma = pltpu.SemaphoreType.DMA
    chips = Z * X
    return pl.pallas_call(
        kernel,
        name="layer",
        out_shape=jax.ShapeDtypeStruct((TOK, D), BF16),
        in_specs=[hbm] * 16,
        out_specs=hbm,
        scratch_shapes=[
            pltpu.VMEM((chips, 8, 2 * ROWS, 128), BF16),
            pltpu.VMEM((C * Y, TOK, D), BF16),
            pltpu.VMEM((Z, CHIP_TOK, 128), BF16),
            pltpu.VMEM((CHIP_TOK, 256), F32),
            pltpu.VMEM((CHIP_TOK, 512), F32),
            pltpu.VMEM((1, D), F32),
            pltpu.VMEM((CONV_W, 256), F32),
            pltpu.VMEM((1, 256), F32),
            pltpu.VMEM((1, 256), F32),
            pltpu.VMEM((1, 256), F32),
            pltpu.VMEM((2, 128), F32),
            pltpu.VMEM((1, 256), F32),
            pltpu.VMEM((2, 8, 128), F32),
            pltpu.VMEM((8, 128), F32),
            pltpu.VMEM((2, 32, 128), BF16),
            pltpu.VMEM((2, 32, 128), BF16),
            pltpu.VMEM((32 + CHIP_TOK, 128), F32),
            pltpu.VMEM((CHIP_TOK, 128), F32),
            pltpu.VMEM((8, CHIP_TOK), F32),
            pltpu.VMEM((C * Y - 1, 8, CHIP_TOK), F32),
            pltpu.VMEM((CHIP_TOK, 128), F32),
            pltpu.VMEM((CHIP_TOK, 128), F32),
            pltpu.VMEM((CHIP_TOK, 128), BF16),
            pltpu.VMEM((CHIP_TOK, 128), F32),
            pltpu.VMEM((4, 128, 128), F32),
            pltpu.VMEM((X, 48, 128), BF16),
            pltpu.VMEM((X, 48, 128), BF16),
            pltpu.VMEM((48, 128), BF16),
            pltpu.VMEM((Z, 48, 128), BF16),
            pltpu.VMEM((X, 32, 128), BF16),
            pltpu.VMEM((X, 32, 128), BF16),
            pltpu.VMEM((CHIP_TOK, 256), BF16),
            pltpu.VMEM((8, 128, 256), BF16),
            pltpu.VMEM((8, 128, 256), BF16),
            pltpu.VMEM((8, Y, TOK, 256), BF16),
            pltpu.VMEM((Y - 1, 8, TOK, 256), BF16),
            pltpu.VMEM((TOK, D), BF16),
            dma((10,)),
            dma((14,)),
            dma((3,)),
            dma((10,)),
            dma((Y,)),
            dma((2, Z // 2 + 1, 3)),
            dma((2, Z)),
            dma((8,)),
            dma((4,)),
        ],
        compiler_params=pltpu.CompilerParams(
            collective_id=0, has_side_effects=True, vmem_limit_bytes=56 * 1024 * 1024
        ),
    )(
        tokens,
        forget_gate_weight,
        recurrence_value_weight,
        output_gate_weight,
        query_projection_weight,
        convolution_value_weight,
        convolution_gate_weight,
        convolution_output_weight.T,
        recurrence_output_weight.T,
        input_norm_gain[None],
        depthwise_filter_taps,
        channel_norm_gain[None],
        channel_norm_bias[None],
        forget_floor_margin[None],
        decay_jump_terms,
        head_norm_gain[None],
    )


def solution(mesh):
    split = Mesh(mesh.devices.reshape(Z, X, C, Y), SP_TP)
    return jax.shard_map(
        per_device,
        mesh=split,
        in_specs=(
            P(SP_TP, None),
            P(),
            P(SP, "tp"),
            P(SP, "tp"),
            P(None, "tp"),
            P("tp"),
            P("tp"),
            P(SP, "tp"),
            P(SP, "tp"),
            P(SP, "tp"),
            P(SP, "tp"),
            P("tp"),
            P("tp", SP),
            P("tp"),
            P("tp", SP),
            P("tp", SP),
        ),
        out_specs=P(SP_TP, None),
        check_vma=False,
    )
```

time: 96.3 us -> 84.9 us (0.88)
  the two profiles are of different devices: /device:TPU:4 before, /device:TPU:1 now
where the time goes in v2:
time: 84.9 us; the launch traced here: 84.8 us
  Pallas kernels  83.2 us (98%)
  local copies, waits for them, and re-layouts  1.57 us (2%)
    pallas_call x1, Pallas kernels, per_device(): pl.pallas_call(kernel, name='layer', out_shape=jax.ShapeDtypeStruct((TOK,...  83.2 us

profile of v2, /device:TPU:1, one launch (start us, length us, event | category | flops | bytes accessed | tf_op | source)
XLA Modules:
  0.0 84.8 jit_solution(10065634639404184570)
XLA Ops:
  0.0 83.2 %layer.1 = bf16[32,2048]{1,0:T(8,128)(2,1)} custom-call(bf16[32,2048]{1,0:T(8,128)(2,1)} %tokens.1, bf16[16,256]{1,0:T(8,128)(2,1)} %w_forget.1, bf16[16,256]{1,0:T(8,128)(2,1)} %w_input.1, bf16[16,256]{1,0:T(8,128)(2,1)} %w_outgate.1, bf16[16,256]{1,0:T(8,128)(2,1)} %w_query.1, bf16[16,256]{1,0:T(8,128)(2,1)} %w_value.1, bf16[16,256]{1,0:T(8,128)(2,1)} %w_gate.1, ...), custom_call_target="tpu_custom_call" | custom-call | tf_op jit(solution)/shard_map/layer/pallas_call | solution.py:470
  83.2 1.6 %copy.18 = bf16[32,2048]{1,0:T(8,128)(2,1)} copy(bf16[32,2048]{1,0:T(8,128)(2,1)} %layer.1) | data formatting | bytes 262144

commit v3 on v2

--- a/solution.py
+++ b/solution.py
@@ -42,9 +42,9 @@
     gain_in, taps_in, cn_gain_in, cn_bias_in, margin_in, jumps_in, head_gain_in,
     out,
     W, Xr, Xn, accs, acc, gain, taps, cn_gain, cn_bias, margin, jumps, head_gain,
-    jbuf, jrecv, hsend, hrecv, gext, conv, stat_s, stat_r, keys, cums, qt, inner, starts,
-    p1s, p1r, p2s, p2r, p3s, p3r, AO, ps, pr, ss, yr, ob,
-    local_sem, one_s, z_s, one_r, ty_r, z_r, xb_r, o_r, y_r,
+    jbuf, jrecv, hsend, hrecv, gext, conv, stat_s, stat_r, wst, keys, cums, qt, inner, starts,
+    p1s, p1r, p2s, p2r, p3s, p3r, AO, wo, ps, pr, po, ss, yr, ob,
+    local_sem, one_s, z_s, one_r, ty_r, xa_r, z_r, xb_r, o_r, y_r,
 ):
     z = lax.axis_index("sp_0")
     x = lax.axis_index("sp_1")
@@ -80,6 +80,9 @@
     mine = c * Y + y
     own_tokens = pltpu.make_async_copy(tokens, Xr.at[mine], local_sem.at[0])
     rows = pl.ds(pl.multiple_of(c * ROWS, ROWS), ROWS)
+    stage = [pltpu.make_async_copy(w, wst.at[m], local_sem.at[10]) for m, w in enumerate(weights)]
+    for copy in stage:
+        copy.start()
     for m, w in enumerate(weights):
         pltpu.make_async_copy(w.at[:, half], W.at[chip, m, rows], local_sem.at[1]).start()
     own_tokens.start()
@@ -93,31 +96,34 @@
     peers = [partner, next_chip, prev_chip]
     peers += [at(dx=d) for d in range(1, X)]
     peers += [at(dy=d) for d in range(1, Y)] + [at(dy=d, dc=1) for d in range(1, Y)]
-    peers += [at(dz=d) for d in range(1, Z)]
+    peers += [at(dz=1), at(dz=-1)]
     for peer in peers:
         pl.semaphore_signal(barrier, inc=1, device_id=peer, device_id_type=MESH)
+    pltpu.make_async_copy(wst, wst, local_sem.at[10]).wait()
+    own_tokens.wait()
     pl.semaphore_wait(barrier, len(peers))
 
-    for m, w in enumerate(weights):
-        send(w.at[:, other_half], W.at[chip, m, rows], one_s.at[0], one_r.at[0], partner).start()
+    part = wst.at[:, :, other_half]
+    send(part, W.at[chip, :, rows], one_s.at[0], one_r.at[0], partner).start()
     for d in range(1, Y):
-        send(tokens, Xr.at[mine], one_s.at[1], ty_r.at[d], at(dy=d)).start()
-    send(tokens, Xr.at[mine], one_s.at[2], one_r.at[1], partner).start()
+        send(Xr.at[mine], Xr.at[mine], one_s.at[1], ty_r.at[d], at(dy=d)).start()
+    send(Xr.at[mine], Xr.at[mine], one_s.at[2], one_r.at[1], partner).start()
     own_rows = W.at[chip, :, rows]
     pltpu.make_async_copy(own_rows, own_rows, local_sem.at[1]).wait()
     arrived(W.at[chip, pl.ds(0, 4)], one_r.at[0])
 
     def z_slot(zo, m):
-        if m == 2:
-            return W.at[zo * X + x, pl.ds(3, 5)]
-        return W.at[pl.ds(zo * X, X), pl.ds(0, 2) if m == 0 else pl.ds(2, 1)]
+        if m >= X:
+            return W.at[zo * X + x, pl.ds(3, 3) if m == X else pl.ds(6, 2)]
+        return W.at[zo * X + lax.rem(x + m, X), pl.ds(0, 3)]
 
     def z_row(way, step):
         return lax.rem(z + Z + step * (1 if way else -1), Z)
 
     def z_copy(way, step, m, zo):
+        sem = z_s.at[0 if m < X else m - X + 1]
         return send(
-            z_slot(zo, m), z_slot(zo, m), z_s.at[m], z_r.at[way, step, m], at(dz=-1 if way else 1)
+            z_slot(zo, m), z_slot(zo, m), sem, z_r.at[way, step, m], at(dz=-1 if way else 1)
         )
 
     def z_send(way, step, m):
@@ -143,16 +149,26 @@
             part = x_half(zo, -dx, side)
             send(part, part, one_s.at[4], one_r.at[2], at(dx=dx)).start()
 
-    for way in range(2):
-        z_send(way, 1, 2)
     slot = W.at[chip, pl.ds(0, 3)]
-    for d in range(1, X):
-        send(slot, slot, one_s.at[5], one_r.at[3], at(dx=d)).start()
-    x_send(z)
-    arrived(W.at[pl.ds(0, 3), pl.ds(0, 3)], one_r.at[3])
-    for m in range(2):
+    for d in (1, X - 1, 2):
+        send(slot, slot, one_s.at[5], xa_r.at[d], at(dx=d)).start()
+    for m in (0, X, X + 1):
         for way in range(2):
             z_send(way, 1, m)
+    x_send(z)
+    for d in (1, X - 1, 2):
+        arrived(W.at[z * X + lax.rem(x + X - d, X), pl.ds(0, 3)], xa_r.at[d])
+        for way in range(2):
+            z_send(way, 1, X - d)
+
+    def norm_body(i, carry):
+        at_row = pl.multiple_of(lax.rem(i, 2) * 16, 16)
+        v = Xr[i // 2, pl.ds(at_row, 16), :].astype(F32)
+        v = v * lax.rsqrt(jnp.mean(v * v, axis=1, keepdims=True) + norm_eps) * gain[...]
+        v = v.astype(BF16)
+        for k in range(Z):
+            Xn[k, pl.ds(pl.multiple_of(i * 16, 16), 16), :] = v[:, k * 128 : (k + 1) * 128]
+        return carry
 
     def row_block(zo, m):
         return W[pl.ds(zo * X, X), m].reshape(128, 128)
@@ -170,14 +186,14 @@
         accs[...] = part if first else accs[...] + part
 
     half_way = Z // 2
-    furthest = ((half_way, half_way - 1, half_way - 1), (half_way - 1, half_way, half_way))
+    far_way = (0, 1, 0, 1, 0, 1)
     for step in range(1, half_way):
-        for m in (0, 2, 1):
+        for m in (0, 4, 3, 5, 1, 2):
             for way in range(2):
                 z_wait(way, step, m)
-                if furthest[way][m] > step:
+                if step + 1 < half_way or far_way[m] == way:
                     z_send(way, step + 1, m)
-                if m == 2:
+                if m == 5:
                     x_send(z_row(way, step))
         for way in range(2):
             if way == 0 or step > 1:
@@ -193,30 +209,20 @@
                 jbuf[h] = jnp.broadcast_to(jumps[h : h + 1, :], (8, 128))
         if step == 2:
             send(jbuf.at[1 - c], jrecv, one_s.at[6], one_r.at[4], partner).start()
-            own_tokens.wait()
             small[0].wait()
             arrived(Xr.at[pl.ds(0, 4)], one_r.at[1])
-
-            def norm_body(i, carry):
-                at_row = pl.multiple_of(lax.rem(i, 2) * 16, 16)
-                v = Xr[i // 2, pl.ds(at_row, 16), :].astype(F32)
-                v = v * lax.rsqrt(jnp.mean(v * v, axis=1, keepdims=True) + norm_eps) * gain[...]
-                v = v.astype(BF16)
-                for k in range(Z):
-                    Xn[k, pl.ds(pl.multiple_of(i * 16, 16), 16), :] = v[:, k * 128 : (k + 1) * 128]
-                return carry
-
-            lax.fori_loop(0, CHIP_TOK // 16, norm_body, 0)
-        if step >= 3:
-            for s in (step, step - 2) if step < 5 else (step,):
-                project_rows(z_row(0, s), z_row(1, s), s == 3)
-
-    z_wait(0, half_way, 0)
-    z_wait(1, half_way, 2)
+        if 2 <= step <= 5:
+            lax.fori_loop(4 * (step - 2), 4 * (step - 1), norm_body, 0)
+        if step >= 6:
+            for s in range(3 * step - 17, 3 * step - 14):
+                project_rows(z_row(0, s), z_row(1, s), s == 1)
+    for m in (0, 4, 3, 5, 1, 2):
+        z_wait(far_way[m], half_way, m)
     far = z_row(0, half_way)
     x_send(far)
     for way in range(2):
         x_forward(z_row(way, half_way - 1))
+    project_rows(z_row(0, half_way - 1), z_row(1, half_way - 1), False)
     project_rows(z, far, False)
 
     arrived(jrecv, one_r.at[4])
@@ -252,20 +258,20 @@
         state = jnp.exp(fin) * state + dot(v, k_f, (0, 0))
         total = total + fin
 
-    upper8 = lax.broadcasted_iota(jnp.int32, (16, 128), 0) < 8
+    upper4 = lax.broadcasted_iota(jnp.int32, (8, 128), 0) < 4
 
     def pack_decay(a):
         hi = a.astype(BF16).astype(F32)
-        return jnp.where(upper8, hi, a - hi).astype(BF16)
+        return jnp.where(upper4, hi, a - hi).astype(BF16)
 
     def unpack_decay(block):
         block = block.astype(F32)
-        return block[0:1] + block[8:9]
+        return block[0:1] + block[4:5]
 
     decay_rows = pack_decay(total)
     for j in range(X):
         p1s[j, 0:32, :] = state[32 * j : 32 * (j + 1)].astype(BF16)
-        p1s[j, 32:48, :] = decay_rows
+        p1s[j, 32:40, :] = decay_rows
     for d in range(1, X):
         send(p1s.at[lax.rem(x + d, X)], p1r.at[x], one_s.at[7], one_r.at[5], at(dx=d)).start()
     x_forward(far)
@@ -276,15 +282,14 @@
     ahead = []
     for j in range(X):
         ahead.append((state_in, decay_in))
-        a = unpack_decay(p1r[j, 32:48, :])
+        a = unpack_decay(p1r[j, 32:40, :])
         state_in = jnp.exp(a) * state_in + p1r[j, 0:32, :].astype(F32)
         decay_in = decay_in + a
     p2s[0:32, :] = state_in.astype(BF16)
-    p2s[32:48, :] = pack_decay(decay_in)
+    p2s[32:40, :] = pack_decay(decay_in)
     for d in range(1, Z):
         send(p2s, p2r.at[z], one_s.at[8], one_r.at[6], at(dz=d)).start()
 
-    z_wait(1, half_way, 1)
     arrived(W.at[pl.ds(0, 10)], one_r.at[2])
 
     def weight_block(k, m):
@@ -349,10 +354,17 @@
                     stat_s, stat_r.at[i - 1], one_s.at[10], one_r.at[8], at(dc=dc, dy=d)
                 ).start()
 
+    def turn_body(n, carry):
+        wo[n, 0:128, :] = weight_block(n, CONV_OUT).T
+        wo[n, 128:256, :] = weight_block(n, REC_OUT).T
+        return carry
+
+    lax.fori_loop(0, 8, turn_body, 0)
+
     arrived(p2r.at[pl.ds(0, Z - 1)], one_r.at[6])
 
     def over_z(zo, carried):
-        a = unpack_decay(p2r[zo, 32:48, :])
+        a = unpack_decay(p2r[zo, 32:40, :])
         return jnp.exp(a) * carried + p2r[zo, 0:32, :].astype(F32)
 
     carried = lax.fori_loop(0, z, over_z, jnp.zeros((32, 128), F32))
@@ -385,18 +397,8 @@
     keep = pl.ds(pl.multiple_of(c * 128, 128), 128)
     give = pl.ds(pl.multiple_of((1 - c) * 128, 128), 128)
 
-    def out_weight(n):
-        return jnp.concatenate([weight_block(n, CONV_OUT), weight_block(n, REC_OUT)], axis=1)
-
     def out_copy(n):
         return send(ps.at[n], pr.at[n], one_s.at[12], o_r.at[n], partner)
-
-    def give_body(n, carry):
-        ps[n] = dot(AO[give, :], out_weight(n), (1, 1)).astype(BF16)
-        out_copy(n).start()
-        return carry
-
-    lax.fori_loop(0, 8, give_body, 0)
 
     def y_copy(g, d):
         part = pl.ds(g * 2, 2)
@@ -404,27 +406,26 @@
             ss.at[part, lax.rem(y + d, Y)], yr.at[d - 1, part], one_s.at[13], y_r.at[g], at(dy=d)
         )
 
-    def keep_body(g, carry):
+    def pair_sum(g):
+        for n in (2 * g, 2 * g + 1):
+            out_copy(n).wait_recv()
+            ss[n] = (po[n] + pr[n].astype(F32)).astype(BF16).reshape(Y, TOK, 256)
+        for d in (2, 1, 3):
+            y_copy(g, d).start()
+
+    def out_body(g, carry):
         for i in range(2):
             n = 2 * g + i
-            kept_part = dot(AO[keep, :], out_weight(n), (1, 1))
-            out_copy(n).wait_recv()
-            ss[n] = (kept_part + pr[n].astype(F32)).astype(BF16).reshape(Y, TOK, 256)
-        for d in (2, 1, 3):
-            y_copy(g, d).start()
+            ps[n] = dot(AO[give, :], wo[n], (1, 0)).astype(BF16)
+            out_copy(n).start()
+            po[n] = dot(AO[keep, :], wo[n], (1, 0))
         return carry
 
-    lax.fori_loop(0, 4, keep_body, 0)
-
     for g in range(4):
-        arrived(yr.at[pl.ds(0, Y - 1), pl.ds(g * 2, 2)], y_r.at[g])
-        for n in (2 * g, 2 * g + 1):
-            mixed = ss[n, y].astype(F32)
-            for d in range(Y - 1):
-                mixed = mixed + yr[d, n].astype(F32)
-            ob[:, n * 256 : (n + 1) * 256] = mixed.astype(BF16)
-        cols = pl.ds(g * 512, 512)
-        pltpu.make_async_copy(ob.at[:, cols], out.at[:, cols], local_sem.at[9]).start()
+        out_body(g, 0)
+        if g:
+            pair_sum(g - 1)
+    pair_sum(3)
 
     left(W.at[0, pl.ds(0, 4)], one_s.at[0])
     left(Xr.at[pl.ds(0, 3)], one_s.at[1])
@@ -438,11 +439,21 @@
     left(hsend, one_s.at[9])
     left(stat_r.at[pl.ds(0, C * Y - 1)], one_s.at[10])
     left(p3s.at[pl.ds(0, X - 1)], one_s.at[11])
+    left(W.at[pl.ds(0, 60), pl.ds(0, 3)], z_s.at[0])
+    left(W.at[pl.ds(0, 15), pl.ds(0, 3)], z_s.at[1])
+    left(W.at[pl.ds(0, 15), pl.ds(0, 2)], z_s.at[2])
+    for g in range(4):
+        arrived(yr.at[pl.ds(0, Y - 1), pl.ds(g * 2, 2)], y_r.at[g])
+        for n in (2 * g, 2 * g + 1):
+            mixed = ss[n, y].astype(F32)
+            for d in range(Y - 1):
+                mixed = mixed + yr[d, n].astype(F32)
+            ob[:, n * 256 : (n + 1) * 256] = mixed.astype(BF16)
+        cols = pl.ds(g * 512, 512)
+        pltpu.make_async_copy(ob.at[:, cols], out.at[:, cols], local_sem.at[9]).start()
+
     left(ps, one_s.at[12])
     left(ss.at[pl.ds(0, 6)], one_s.at[13])
-    left(W.at[pl.ds(0, 15)], z_s.at[0])
-    left(W.at[pl.ds(0, 15), pl.ds(0, 4)], z_s.at[1])
-    left(W.at[pl.ds(0, 15), pl.ds(0, 5)], z_s.at[2])
     pltpu.make_async_copy(ob, out, local_sem.at[9]).wait()
 
 
@@ -494,29 +505,33 @@
             pltpu.VMEM((CHIP_TOK, 128), F32),
             pltpu.VMEM((8, CHIP_TOK), F32),
             pltpu.VMEM((C * Y - 1, 8, CHIP_TOK), F32),
+            pltpu.VMEM((8, ROWS, 256), BF16),
             pltpu.VMEM((CHIP_TOK, 128), F32),
             pltpu.VMEM((CHIP_TOK, 128), F32),
             pltpu.VMEM((CHIP_TOK, 128), BF16),
             pltpu.VMEM((CHIP_TOK, 128), F32),
             pltpu.VMEM((4, 128, 128), F32),
-            pltpu.VMEM((X, 48, 128), BF16),
-            pltpu.VMEM((X, 48, 128), BF16),
-            pltpu.VMEM((48, 128), BF16),
-            pltpu.VMEM((Z, 48, 128), BF16),
+            pltpu.VMEM((X, 40, 128), BF16),
+            pltpu.VMEM((X, 40, 128), BF16),
+            pltpu.VMEM((40, 128), BF16),
+            pltpu.VMEM((Z, 40, 128), BF16),
             pltpu.VMEM((X, 32, 128), BF16),
             pltpu.VMEM((X, 32, 128), BF16),
             pltpu.VMEM((CHIP_TOK, 256), BF16),
+            pltpu.VMEM((8, 256, 256), BF16),
             pltpu.VMEM((8, 128, 256), BF16),
             pltpu.VMEM((8, 128, 256), BF16),
+            pltpu.VMEM((8, 128, 256), F32),
             pltpu.VMEM((8, Y, TOK, 256), BF16),
             pltpu.VMEM((Y - 1, 8, TOK, 256), BF16),
             pltpu.VMEM((TOK, D), BF16),
-            dma((10,)),
+            dma((11,)),
             dma((14,)),
             dma((3,)),
             dma((10,)),
             dma((Y,)),
-            dma((2, Z // 2 + 1, 3)),
+            dma((X,)),
+            dma((2, Z // 2 + 1, 6)),
             dma((2, Z)),
             dma((8,)),
             dma((4,)),

time: 84.9 us -> 77.8 us (0.916)
  Pallas kernels: 83.2 us -> 76.1 us
    pallas_call x1, Pallas kernels: 83.2 us -> 76.1 us  [per_device(): pl.pallas_call(kernel, name='layer', out_shape=jax.ShapeDtypeStruct((TOK,...]
where the time goes in v3:
time: 77.8 us; the launch traced here: 77.7 us
  Pallas kernels  76.1 us (98%)
  local copies, waits for them, and re-layouts  1.57 us (2%)
    pallas_call x1, Pallas kernels, per_device(): pl.pallas_call(kernel, name='layer', out_shape=jax.ShapeDtypeStruct((TOK,...  76.1 us
    unnamed x1, local copies, waits for them, and re-layouts  1.57 us

profile of v3, /device:TPU:1, one launch (start us, length us, event | category | flops | bytes accessed | tf_op | source)
XLA Modules:
  0.0 77.7 jit_solution(342337089320120399)
XLA Ops:
  0.0 76.1 %layer.1 = bf16[32,2048]{1,0:T(8,128)(2,1)} custom-call(bf16[32,2048]{1,0:T(8,128)(2,1)} %tokens.1, bf16[16,256]{1,0:T(8,128)(2,1)} %w_forget.1, bf16[16,256]{1,0:T(8,128)(2,1)} %w_input.1, bf16[16,256]{1,0:T(8,128)(2,1)} %w_outgate.1, bf16[16,256]{1,0:T(8,128)(2,1)} %w_query.1, bf16[16,256]{1,0:T(8,128)(2,1)} %w_value.1, bf16[16,256]{1,0:T(8,128)(2,1)} %w_gate.1, ...), custom_call_target="tpu_custom_call" | custom-call | tf_op jit(solution)/shard_map/layer/pallas_call | solution.py:481
  76.1 1.6 %copy.18 = bf16[32,2048]{1,0:T(8,128)(2,1)} copy(bf16[32,2048]{1,0:T(8,128)(2,1)} %layer.1) | data formatting | bytes 262144
